TPU v7x, 32 devices: a whole 2x2x4 slice. The times are simulated.
32 devices in a mesh: grp: 1, fs: 2 (over x), tp: 16 (over z, y, core).
Axes of the slice: x: 2, y: 2, z: 4, core: 2. Of those that a mesh axis runs over, the one named last changes fastest.
Arguments:
- prompt_rows: bfloat16 [512, 2048], P(('grp', 'fs')), may hold values from -6 to 6
- gain_before: float32 [2048], P('fs'), may hold values from 0.1 to 1.9
- gate_before: float32 [2048, 5632], P('fs', 'tp'), may hold values from -0.125 to 0.125
- up_before: float32 [2048, 5632], P('fs', 'tp'), may hold values from -0.125 to 0.125
- down_before: float32 [5632, 2048], P('fs', 'tp'), may hold values from -0.3125 to 0.3125
- gain_after: float32 [2048], P('fs'), may hold values from 0.1 to 1.9
- gate_after: float32 [2048, 5632], P('fs', 'tp'), may hold values from -0.125 to 0.125
- up_after: float32 [2048, 5632], P('fs', 'tp'), may hold values from -0.125 to 0.125
- down_after: float32 [5632, 2048], P('fs', 'tp'), may hold values from -0.3125 to 0.3125
Outputs:
- mixed_rows: bfloat16 [512, 2048], P(('grp', 'fs'))
- served_gate_before: bfloat16 [2048, 5632], P('grp', 'tp')
- served_up_before: bfloat16 [2048, 5632], P('grp', 'tp')
- served_down_before: bfloat16 [5632, 2048], P(('grp', 'tp'))
- served_gate_after: bfloat16 [2048, 5632], P('grp', 'tp')
- served_up_after: bfloat16 [2048, 5632], P('grp', 'tp')
- served_down_after: bfloat16 [5632, 2048], P(('grp', 'tp'))
All inputs are finite; a program needn't handle non-finite values.
Results may differ from a plain program's by a relative error of at most 0.03.
Values may be sent and summed in bfloat16 or wider, within the bound.
No kernel may reach another device: no remote copies, remote signals or barrier semaphores. Data moves between devices by JAX's collectives and lax.ppermute only.
A program may use at most 64 MiB of HBM per device.

v0:
```python
import jax
import jax.numpy as jnp
from jax import lax
from jax.sharding import PartitionSpec as P

EPS = 1e-06


def serve_weights(gain, gate_w, up_w, down_w):
    gate_half = (gain[:, None] * gate_w).astype(jnp.bfloat16)
    up_half = (gain[:, None] * up_w).astype(jnp.bfloat16)
    down_half = down_w.astype(jnp.bfloat16)
    gate_whole, up_whole = (
        lax.all_gather(gate_half, "fs", axis=0, tiled=True),
        lax.all_gather(up_half, "fs", axis=0, tiled=True),
    )
    tall_block = lax.all_gather(down_half, "fs", axis=0, tiled=True)
    down_whole = lax.all_to_all(tall_block, "tp", split_axis=0, concat_axis=1, tiled=True)
    return (gate_whole, up_whole, down_whole)


def half_step(row_block, gate_w, up_w, down_w):
    values = row_block.astype(jnp.float32)
    normed = (values * lax.rsqrt(jnp.mean(values * values, axis=-1, keepdims=True) + EPS)).astype(
        jnp.bfloat16
    )
    gate_pre = jnp.dot(normed, gate_w, preferred_element_type=jnp.float32)
    up_pre = jnp.dot(normed, up_w, preferred_element_type=jnp.float32)
    hidden = (jax.nn.silu(gate_pre) * up_pre).astype(jnp.bfloat16)
    total = lax.psum(
        jnp.dot(hidden, down_w, preferred_element_type=jnp.float32).astype(jnp.bfloat16), "tp"
    ).astype(jnp.float32)
    return (values + 0.5 * total).astype(jnp.bfloat16)


def body(
    prompt_rows,
    gain_before,
    gate_before,
    up_before,
    down_before,
    gain_after,
    gate_after,
    up_after,
    down_after,
):
    gate_one, up_one, down_one = serve_weights(gain_before, gate_before, up_before, down_before)
    gate_two, up_two, down_two = serve_weights(gain_after, gate_after, up_after, down_after)
    middle = half_step(prompt_rows, gate_one, up_one, down_one)
    mixed = half_step(middle, gate_two, up_two, down_two)
    return (mixed, gate_one, up_one, down_one, gate_two, up_two, down_two)


def solution(mesh):
    placed = (
        P(("grp", "fs"), None),
        P("fs"),
        P("fs", "tp"),
        P("fs", "tp"),
        P("fs", "tp"),
        P("fs"),
        P("fs", "tp"),
        P("fs", "tp"),
        P("fs", "tp"),
    )
    return jax.shard_map(
        body,
        mesh=mesh,
        in_specs=placed,
        out_specs=(
            P(("grp", "fs"), None),
            P("grp", "tp"),
            P("grp", "tp"),
            P(("grp", "tp"), None),
            P("grp", "tp"),
            P("grp", "tp"),
            P(("grp", "tp"), None),
        ),
        check_vma=False,
    )
```

profile of v0, /device:TPU:0, one launch (start us, length us, event | category | flops | bytes accessed | tf_op | source)
XLA Modules:
  0.0 390.6 jit_solution(4047119397556258142)
XLA Ops:
  7.2 2.4 convert_element_type.59
  9.8 2.2 multiply_convert_fusion.3
  12.0 26.6 %all-gather.11.cloned.1.call-done = bf16[5632,128]{1,0:T(8,128)(2,1)} async-done(((bf16[2816,128]{1,0:T(8,128)(2,1)}), bf16[5632,128]{1,0:T(8,128)(2,1)}) %all-gather.11.cloned.1.call-update) | async-done | bytes 1441808 | tf_op jit(solution)/shard_map/all_gather | solution.py:17
  38.6 5.6 %all-to-all-start = ((bf16[16,352,128]{2,1,0:T(8,128)(2,1)}), bf16[16,352,128]{2,1,0:T(8,128)(2,1)S(1)}, u32[]{:S(2)}, u32[]{:S(2)}) async-start(bf16[16,352,128]{2,1,0:T(8,128)(2,1)} %bitcast.21), calls=%async_computation | async-start | bytes 2883584 | tf_op jit(solution)/shard_map/all_to_all | solution.py:18
  44.3 2.4 convert_element_type.68
  47.5 18.9 %all-gather.7.cloned.1.call-done = bf16[2048,352]{0,1:T(8,128)(2,1)} async-done(((bf16[1024,352]{0,1:T(8,128)(2,1)}), bf16[2048,352]{0,1:T(8,128)(2,1)}) %all-gather.7.cloned.1.call-update) | async-done | bytes 1441808 | tf_op jit(solution)/shard_map/all_gather | solution.py:14
  66.4 2.0 fusion.14
  68.5 25.8 %all-gather.17.cloned.1.call-done = bf16[5632,128]{1,0:T(8,128)(2,1)} async-done(((bf16[2816,128]{1,0:T(8,128)(2,1)}), bf16[5632,128]{1,0:T(8,128)(2,1)}) %all-gather.17.cloned.1.call-update) | async-done | bytes 1441808 | tf_op jit(solution)/shard_map/all_gather | solution.py:17
  94.3 5.6 %all-to-all-start.1 = ((bf16[16,352,128]{2,1,0:T(8,128)(2,1)}), bf16[16,352,128]{2,1,0:T(8,128)(2,1)S(1)}, u32[]{:S(2)}, u32[]{:S(2)}) async-start(bf16[16,352,128]{2,1,0:T(8,128)(2,1)} %bitcast.20), calls=%async_computation.1 | async-start | bytes 2883584 | tf_op jit(solution)/shard_map/all_to_all | solution.py:18
  100.0 1.3 copy_bitcast_fusion.1
  101.3 20.7 %all-gather.9.cloned.1.call-done = bf16[2048,352]{0,1:T(8,128)(2,1)} async-done(((bf16[1024,352]{0,1:T(8,128)(2,1)}), bf16[2048,352]{0,1:T(8,128)(2,1)}) %all-gather.9.cloned.1.call-update) | async-done | bytes 1441808 | tf_op jit(solution)/shard_map/all_gather | solution.py:15
  122.0 5.3 %convolution_convert_fusion.1 = bf16[256,2048]{1,0:T(8,128)(2,1)} fusion(bf16[352,2048]{1,0:T(8,128)(2,1)} %copy_bitcast_fusion.1, bf16[2048,352]{0,1:T(8,128)(2,1)} %all-gather.9.cloned.1.call-done, bf16[256,2048]{1,0:T(8,128)(2,1)} %param.9, f32[256]{0:T(256)S(1)} %add_rsqrt_fusion.1, f32[256,352]{0,1:T(8,128)S(1)} %fusion.14), kind=kOutput, calls=%fused_computation.7 | convolution fusion | flops 740835328 | bytes 5342208 | tf_op jit(solution)/shard_map/dot_general | solution.py:31
  127.4 2.8 multiply_convert_fusion.1
  131.1 1.3 copy_bitcast_fusion
  132.4 89.0 %all-reduce.3.cloned.1.call-done = bf16[256,2048]{1,0:T(8,128)(2,1)} async-done(((bf16[256,2048]{1,0:T(8,128)(2,1)}), bf16[256,2048]{1,0:T(8,128)(2,1)}) %all-reduce.3.cloned.1.call-update) | async-done | bytes 1048592 | tf_op jit(solution)/shard_map/psum | solution.py:30
  221.3 1.8 fusion.3
  223.2 25.0 %all-gather.13.cloned.1.call-done = bf16[2048,352]{0,1:T(8,128)(2,1)} async-done(((bf16[1024,352]{0,1:T(8,128)(2,1)}), bf16[2048,352]{0,1:T(8,128)(2,1)}) %all-gather.13.cloned.1.call-update) | async-done | bytes 1441808 | tf_op jit(solution)/shard_map/all_gather | solution.py:14
  248.1 2.1 fusion.10
  250.3 25.7 %all-gather.15.cloned.1.call-done = bf16[2048,352]{0,1:T(8,128)(2,1)} async-done(((bf16[1024,352]{0,1:T(8,128)(2,1)}), bf16[2048,352]{0,1:T(8,128)(2,1)}) %all-gather.15.cloned.1.call-update) | async-done | bytes 1441808 | tf_op jit(solution)/shard_map/all_gather | solution.py:15
  276.0 4.4 %convolution_convert_fusion = bf16[256,2048]{1,0:T(8,128)(2,1)} fusion(bf16[352,2048]{1,0:T(8,128)(2,1)S(1)} %copy-done.9, bf16[2048,352]{0,1:T(8,128)(2,1)} %all-gather.15.cloned.1.call-done, bf16[256,2048]{1,0:T(8,128)(2,1)S(1)} %get-tuple-element.8, f32[256]{0:T(256)S(1)} %add_rsqrt_fusion, f32[256,352]{0,1:T(8,128)S(1)} %fusion.10), kind=kOutput, calls=%fused_computation.6 | convolution fusion | flops 740835328 | bytes 5342208 | tf_op jit(solution)/shard_map/dot_general | solution.py:31
  280.5 94.0 %all-reduce.5.cloned.1.call-done = bf16[256,2048]{1,0:T(8,128)(2,1)} async-done(((bf16[256,2048]{1,0:T(8,128)(2,1)}), bf16[256,2048]{1,0:T(8,128)(2,1)}) %all-reduce.5.cloned.1.call-update) | async-done | bytes 1048592 | tf_op jit(solution)/shard_map/psum | solution.py:30
  374.4 2.6 fusion.5
  377.0 1.1 copy.30
  378.9 1.1 copy.31
  (45 shorter events, 6.5 us)
Async XLA Ops:
  7.2 2.6 copy-start.2
  7.2 2.6 copy-start.3
  7.2 31.4 %all-gather.11.cloned.1.call-start = ((), (), s32[]{:S(2)}) async-start(), calls=%async_computation.4 | async-start | bytes 2162688 | tf_op jit(solution)/shard_map/all_gather | solution.py:17
  9.7 56.7 %all-gather.7.cloned.1.call-start = ((), (), s32[]{:S(2)}) async-start(), calls=%async_computation.2 | async-start | bytes 2162688 | tf_op jit(solution)/shard_map/all_gather | solution.py:14
  38.6 55.7 %all-to-all-start = ((bf16[16,352,128]{2,1,0:T(8,128)(2,1)}), bf16[16,352,128]{2,1,0:T(8,128)(2,1)S(1)}, u32[]{:S(2)}, u32[]{:S(2)}) async-start(bf16[16,352,128]{2,1,0:T(8,128)(2,1)} %bitcast.21), calls=%async_computation | async-start | bytes 2883584 | tf_op jit(solution)/shard_map/all_to_all | solution.py:18
  44.2 3.0 copy-start
  44.2 50.1 %all-gather.17.cloned.1.call-start = ((), (), s32[]{:S(2)}) async-start(), calls=%async_computation.8 | async-start | bytes 2162688 | tf_op jit(solution)/shard_map/all_gather | solution.py:17
  46.7 75.4 %all-gather.9.cloned.1.call-start = ((), (), s32[]{:S(2)}) async-start(), calls=%async_computation.3 | async-start | bytes 2162688 | tf_op jit(solution)/shard_map/all_gather | solution.py:15
  94.3 36.8 %all-to-all-start.1 = ((bf16[16,352,128]{2,1,0:T(8,128)(2,1)}), bf16[16,352,128]{2,1,0:T(8,128)(2,1)S(1)}, u32[]{:S(2)}, u32[]{:S(2)}) async-start(bf16[16,352,128]{2,1,0:T(8,128)(2,1)} %bitcast.20), calls=%async_computation.1 | async-start | bytes 2883584 | tf_op jit(solution)/shard_map/all_to_all | solution.py:18
  99.9 121.4 %all-reduce.3.cloned.1.call-start = ((), (), s32[]{:S(2)}) async-start(), calls=%async_computation.5 | async-start | bytes 2097152 | tf_op jit(solution)/shard_map/psum | solution.py:30
  101.3 26.1 %copy-start.10 = (f32[1024]{0:T(1024)S(1)}, f32[1024]{0:T(1024)}, u32[]{:S(2)}) copy-start(f32[1024]{0:T(1024)} %param.14) | copy-start | bytes 12292
  122.0 5.4 %copy-start.4 = (f32[1024,352]{0,1:T(8,128)S(1)}, f32[1024,352]{0,1:T(8,128)}, u32[]{:S(2)}) copy-start(f32[1024,352]{0,1:T(8,128)} %param.15) | copy-start | bytes 4325380
  127.3 120.8 %all-gather.13.cloned.1.call-start = ((), (), s32[]{:S(2)}) async-start(), calls=%async_computation.6 | async-start | bytes 2162688 | tf_op jit(solution)/shard_map/all_gather | solution.py:14
  130.3 145.7 %all-gather.15.cloned.1.call-start = ((), (), s32[]{:S(2)}) async-start(), calls=%async_computation.7 | async-start | bytes 2162688 | tf_op jit(solution)/shard_map/all_gather | solution.py:15
  131.0 90.3 %copy-start.1 = (bf16[256,2048]{1,0:T(8,128)(2,1)S(1)}, bf16[256,2048]{1,0:T(8,128)(2,1)}, u32[]{:S(2)}) copy-start(bf16[256,2048]{1,0:T(8,128)(2,1)} %param.9) | copy-start | bytes 3145732
  131.0 243.4 %all-reduce.5.cloned.1.call-start = ((), (), s32[]{:S(2)}) async-start(), calls=%async_computation.9 | async-start | bytes 2097152 | tf_op jit(solution)/shard_map/psum | solution.py:30
  248.1 27.9 %copy-start.9 = (bf16[352,2048]{1,0:T(8,128)(2,1)S(1)}, bf16[352,2048]{1,0:T(8,128)(2,1)}, u32[]{:S(2)}) copy-start(bf16[352,2048]{1,0:T(8,128)(2,1)} %copy_bitcast_fusion) | copy-start | bytes 4325380
  280.5 96.6 %copy-start.5 = (bf16[2048,352]{0,1:T(8,128)(2,1)S(1)}, bf16[2048,352]{0,1:T(8,128)(2,1)}, u32[]{:S(2)}) copy-start(bf16[2048,352]{0,1:T(8,128)(2,1)} %all-gather.7.cloned.1.call-done) | copy-start | bytes 4325380
  377.0 1.9 copy-start.6
  378.9 1.9 copy-start.7
  380.8 1.9 copy-start.8
Sparse Core Ops, SparseCore 0:
  10.1 28.4 all-gather.10
  40.7 25.6 all-gather.6
  68.6 25.6 all-gather.16
  96.3 25.6 all-gather.8
  127.5 93.8 all-reduce.2
  223.3 24.7 all-gather.12
  250.3 25.6 all-gather.14
  280.6 93.8 all-reduce.4
where the time goes:
time: 391 us
  waiting for transfers between devices  327 us (84%)
  other arithmetic  14.5 us (4%)
  between operations  14.3 us (4%)
  matrix products  13.9 us (4%)
  starting transfers between devices  11.6 us (3%)
  local copies, waits for them, and re-layouts  9.35 us (2%)
    psum x2, waiting for transfers between devices, half_step(): lax.psum(jnp.dot(hidden, down_w, preferred_element_type=jnp.float32).asty...  183 us
    all_gather x2, waiting for transfers between devices, serve_weights(): tall_block = lax.all_gather(down_half, 'fs', axis=0, tiled=True)  52.5 us
    all_gather x2, waiting for transfers between devices, serve_weights(): lax.all_gather(up_half, 'fs', axis=0, tiled=True)  46.5 us
    all_gather x2, waiting for transfers between devices, serve_weights(): lax.all_gather(gate_half, 'fs', axis=0, tiled=True)  43.9 us
    all_to_all x2, starting transfers between devices, serve_weights(): lax.all_to_all(tall_block, 'tp', split_axis=0, concat_axis=1, tiled=True)  11.2 us
    dot_general x2, matrix products, half_step(): jnp.dot(hidden, down_w, preferred_element_type=jnp.float32)  9.75 us
  transfers between devices with their start and end apart: 10, of which 8 were waited for; matrix products, arithmetic and copies ran while one was open for 5% of the time, Pallas kernels for 0%

commit v1 on v0

--- a/solution.py
+++ b/solution.py
@@ -4,6 +4,12 @@
 from jax.sharding import PartitionSpec as P
 
 EPS = 1e-06
+
+
+def add_all(value, name):
+    blocks = lax.all_gather(value, name, axis=0, tiled=False)
+    acc = blocks.sum(axis=0)
+    return acc
 
 
 def serve_weights(gain, gate_w, up_w, down_w):
@@ -27,7 +33,7 @@
     gate_pre = jnp.dot(normed, gate_w, preferred_element_type=jnp.float32)
     up_pre = jnp.dot(normed, up_w, preferred_element_type=jnp.float32)
     hidden = (jax.nn.silu(gate_pre) * up_pre).astype(jnp.bfloat16)
-    total = lax.psum(
+    total = add_all(
         jnp.dot(hidden, down_w, preferred_element_type=jnp.float32).astype(jnp.bfloat16), "tp"
     ).astype(jnp.float32)
     return (values + 0.5 * total).astype(jnp.bfloat16)

time: 391 us -> 486 us (1.24)
  waiting for transfers between devices: 327 us -> 405 us
  other arithmetic: 14.5 us -> 31.2 us
    all_gather x0 -> x2, waiting for transfers between devices: none -> 226 us  [add_all(): blocks = lax.all_gather(value, name, axis=0, tiled=False)]
    psum x2 -> x0, waiting for transfers between devices: 183 us -> none  [half_step(): lax.psum(jnp.dot(hidden, down_w, preferred_element_type=jnp.float32).asty...]
    all_to_all x2, waiting for transfers between devices: 0.01 us -> 48.7 us  [serve_weights(): lax.all_to_all(tall_block, 'tp', split_axis=0, concat_axis=1, tiled=True)]
    reduce_sum x0 -> x2, other arithmetic: none -> 18.7 us  [add_all(): acc = blocks.sum(axis=0)]
    all_gather x2, waiting for transfers between devices: 43.9 us -> 34.5 us  [serve_weights(): lax.all_gather(gate_half, 'fs', axis=0, tiled=True)]
  transfers between devices with their start and end apart: 10 -> 10, of which waited for: 8 -> 10; matrix products, arithmetic and copies ran while one was open for 5% -> 6% of each run, Pallas kernels for 0% -> 0%
where the time goes in v1:
time: 486 us; the launch traced here: 485 us
  waiting for transfers between devices  405 us (83%)
  other arithmetic  31.2 us (6%)
  between operations  14.3 us (3%)
  matrix products  13.4 us (3%)
  starting transfers between devices  11.7 us (2%)
  local copies, waits for them, and re-layouts  9.38 us (2%)
    all_gather x2, waiting for transfers between devices, add_all(): blocks = lax.all_gather(value, name, axis=0, tiled=False)  226 us
    all_gather x2, waiting for transfers between devices, serve_weights(): tall_block = lax.all_gather(down_half, 'fs', axis=0, tiled=True)  49.5 us
    all_to_all x2, waiting for transfers between devices, serve_weights(): lax.all_to_all(tall_block, 'tp', split_axis=0, concat_axis=1, tiled=True)  48.7 us
    all_gather x2, waiting for transfers between devices, serve_weights(): lax.all_gather(up_half, 'fs', axis=0, tiled=True)  45 us
    all_gather x2, waiting for transfers between devices, serve_weights(): lax.all_gather(gate_half, 'fs', axis=0, tiled=True)  34.5 us
    reduce_sum x2, other arithmetic, add_all(): acc = blocks.sum(axis=0)  18.7 us
    all_to_all x2, starting transfers between devices, serve_weights(): lax.all_to_all(tall_block, 'tp', split_axis=0, concat_axis=1, tiled=True)  11.4 us
  transfers between devices with their start and end apart: 10, of which 10 were waited for; matrix products, arithmetic and copies ran while one was open for 6% of the time, Pallas kernels for 0%

profile of v1, /device:TPU:0, one launch (start us, length us, event | category | flops | bytes accessed | tf_op | source)
XLA Modules:
  0.0 484.7 jit_solution(3072749329134350362)
XLA Ops:
  7.2 2.4 convert_element_type.63
  9.8 2.2 multiply_convert_fusion.3
  12.0 26.6 %all-gather.15.cloned.1.call-done = bf16[5632,128]{1,0:T(8,128)(2,1)} async-done(((bf16[2816,128]{1,0:T(8,128)(2,1)}), bf16[5632,128]{1,0:T(8,128)(2,1)}) %all-gather.15.cloned.1.call-update) | async-done | bytes 1441808 | tf_op jit(solution)/shard_map/all_gather | solution.py:23
  38.6 5.6 %all-to-all-start = ((bf16[16,352,128]{2,1,0:T(8,128)(2,1)}), bf16[16,352,128]{2,1,0:T(8,128)(2,1)S(1)}, u32[]{:S(2)}, u32[]{:S(2)}) async-start(bf16[16,352,128]{2,1,0:T(8,128)(2,1)} %bitcast.25), calls=%async_computation | async-start | bytes 2883584 | tf_op jit(solution)/shard_map/all_to_all | solution.py:24
  45.0 2.4 convert_element_type.72
  47.8 18.7 %all-gather.11.cloned.1.call-done = bf16[2048,352]{0,1:T(8,128)(2,1)} async-done(((bf16[1024,352]{0,1:T(8,128)(2,1)}), bf16[2048,352]{0,1:T(8,128)(2,1)}) %all-gather.11.cloned.1.call-update) | async-done | bytes 1441808 | tf_op jit(solution)/shard_map/all_gather | solution.py:20
  66.4 2.0 fusion.14
  68.5 5.3 %all-to-all-done = bf16[16,352,128]{2,1,0:T(8,128)(2,1)S(1)} async-done(((bf16[16,352,128]{2,1,0:T(8,128)(2,1)}), bf16[16,352,128]{2,1,0:T(8,128)(2,1)S(1)}, u32[]{:S(2)}, u32[]{:S(2)}) %all-to-all-start) | async-done | bytes 1441824 | tf_op jit(solution)/shard_map/all_to_all | solution.py:24
  73.8 1.3 copy_bitcast_fusion.1
  75.1 19.2 %all-gather.13.cloned.1.call-done = bf16[2048,352]{0,1:T(8,128)(2,1)} async-done(((bf16[1024,352]{0,1:T(8,128)(2,1)}), bf16[2048,352]{0,1:T(8,128)(2,1)}) %all-gather.13.cloned.1.call-update) | async-done | bytes 1441808 | tf_op jit(solution)/shard_map/all_gather | solution.py:21
  94.3 4.9 %convolution_convert_fusion.1 = bf16[256,2048]{1,0:T(8,128)(2,1)} fusion(bf16[352,2048]{1,0:T(8,128)(2,1)} %copy_bitcast_fusion.1, bf16[2048,352]{0,1:T(8,128)(2,1)} %all-gather.13.cloned.1.call-done, bf16[256,2048]{1,0:T(8,128)(2,1)S(1)} %copy-done, f32[256]{0:T(256)S(1)} %add_rsqrt_fusion.1, f32[256,352]{0,1:T(8,128)S(1)} %fusion.14), kind=kOutput, calls=%fused_computation.7 | convolution fusion | flops 740835328 | bytes 5342208 | tf_op jit(solution)/shard_map/dot_general | solution.py:37
  99.2 22.8 %all-gather.21.cloned.1.call-done = bf16[5632,128]{1,0:T(8,128)(2,1)} async-done(((bf16[2816,128]{1,0:T(8,128)(2,1)}), bf16[5632,128]{1,0:T(8,128)(2,1)}) %all-gather.21.cloned.1.call-update) | async-done | bytes 1441808 | tf_op jit(solution)/shard_map/all_gather | solution.py:23
  122.0 5.8 %all-to-all-start.1 = ((bf16[16,352,128]{2,1,0:T(8,128)(2,1)}), bf16[16,352,128]{2,1,0:T(8,128)(2,1)S(1)}, u32[]{:S(2)}, u32[]{:S(2)}) async-start(bf16[16,352,128]{2,1,0:T(8,128)(2,1)} %bitcast.24), calls=%async_computation.1 | async-start | bytes 2883584 | tf_op jit(solution)/shard_map/all_to_all | solution.py:24
  127.8 3.3 multiply_convert_fusion.1
  131.9 43.4 %all-to-all-done.1 = bf16[16,352,128]{2,1,0:T(8,128)(2,1)S(1)} async-done(((bf16[16,352,128]{2,1,0:T(8,128)(2,1)}), bf16[16,352,128]{2,1,0:T(8,128)(2,1)S(1)}, u32[]{:S(2)}, u32[]{:S(2)}) %all-to-all-start.1) | async-done | bytes 1441824 | tf_op jit(solution)/shard_map/all_to_all | solution.py:24
  176.6 99.0 %all-gather.23.cloned.1.call-done = bf16[4096,2048]{1,0:T(8,128)(2,1)} async-done(((bf16[256,2048]{1,0:T(8,128)(2,1)}), bf16[4096,2048]{1,0:T(8,128)(2,1)}) %all-gather.23.cloned.1.call-update) | async-done | bytes 16777232 | tf_op jit(solution)/shard_map/all_gather | solution.py:10
  275.7 9.5 %reduce_sum.43 = bf16[256,2048]{1,0:T(8,128)(2,1)S(1)} reduce(bf16[16,256,2048]{2,1,0:T(8,128)(2,1)} %bitcast.22, bf16[]{:T(256)} %constant.15.clone.1), dimensions={0}, to_apply=%region_1.2 | reduce | flops 7864320 | bytes 17825794 | tf_op jit(solution)/shard_map/reduce_sum | solution.py:11
  285.7 15.8 %all-gather.17.cloned.1.call-done = bf16[2048,352]{0,1:T(8,128)(2,1)} async-done(((bf16[1024,352]{0,1:T(8,128)(2,1)}), bf16[2048,352]{0,1:T(8,128)(2,1)}) %all-gather.17.cloned.1.call-update) | async-done | bytes 1441808 | tf_op jit(solution)/shard_map/all_gather | solution.py:20
  301.5 2.1 fusion.10
  303.7 25.7 %all-gather.19.cloned.1.call-done = bf16[2048,352]{0,1:T(8,128)(2,1)} async-done(((bf16[1024,352]{0,1:T(8,128)(2,1)}), bf16[2048,352]{0,1:T(8,128)(2,1)}) %all-gather.19.cloned.1.call-update) | async-done | bytes 1441808 | tf_op jit(solution)/shard_map/all_gather | solution.py:21
  329.4 4.4 convolution_convert_fusion
  333.9 126.6 %all-gather.25.cloned.1.call-done = bf16[4096,2048]{1,0:T(8,128)(2,1)} async-done(((bf16[256,2048]{1,0:T(8,128)(2,1)}), bf16[4096,2048]{1,0:T(8,128)(2,1)}) %all-gather.25.cloned.1.call-update) | async-done | bytes 16777232 | tf_op jit(solution)/shard_map/all_gather | solution.py:10
  460.5 9.3 %reduce_sum.45 = bf16[256,2048]{1,0:T(8,128)(2,1)S(1)} reduce(bf16[16,256,2048]{2,1,0:T(8,128)(2,1)} %bitcast.23, bf16[]{:T(256)} %constant.15.clone.1), dimensions={0}, to_apply=%region_3.4 | reduce | flops 7864320 | bytes 17825794 | tf_op jit(solution)/shard_map/reduce_sum | solution.py:11
  469.7 1.4 fusion.5
  (43 shorter events, 10.8 us)
Async XLA Ops:
  7.2 2.6 copy-start.2
  7.2 2.6 copy-start.1
  7.2 31.4 %all-gather.15.cloned.1.call-start = ((), (), s32[]{:S(2)}) async-start(), calls=%async_computation.4 | async-start | bytes 2162688 | tf_op jit(solution)/shard_map/all_gather | solution.py:23
  9.7 56.7 %all-gather.11.cloned.1.call-start = ((), (), s32[]{:S(2)}) async-start(), calls=%async_computation.2 | async-start | bytes 2162688 | tf_op jit(solution)/shard_map/all_gather | solution.py:20
  38.6 35.2 %all-to-all-start = ((bf16[16,352,128]{2,1,0:T(8,128)(2,1)}), bf16[16,352,128]{2,1,0:T(8,128)(2,1)S(1)}, u32[]{:S(2)}, u32[]{:S(2)}) async-start(bf16[16,352,128]{2,1,0:T(8,128)(2,1)} %bitcast.25), calls=%async_computation | async-start | bytes 2883584 | tf_op jit(solution)/shard_map/all_to_all | solution.py:24
  44.2 50.1 %all-gather.13.cloned.1.call-start = ((), (), s32[]{:S(2)}) async-start(), calls=%async_computation.3 | async-start | bytes 2162688 | tf_op jit(solution)/shard_map/all_gather | solution.py:21
  44.9 2.5 copy-start
  45.0 77.1 %all-gather.21.cloned.1.call-start = ((), (), s32[]{:S(2)}) async-start(), calls=%async_computation.7 | async-start | bytes 2162688 | tf_op jit(solution)/shard_map/all_gather | solution.py:23
  47.4 228.3 %all-gather.23.cloned.1.call-start = ((), (), s32[]{:S(2)}) async-start(), calls=%async_computation.8 | async-start | bytes 17825792 | tf_op jit(solution)/shard_map/all_gather | solution.py:10
  122.0 5.8 %copy-start.8 = (f32[1024]{0:T(1024)S(1)}, f32[1024]{0:T(1024)}, u32[]{:S(2)}) copy-start(f32[1024]{0:T(1024)} %param.14) | copy-start | bytes 12292
  122.0 53.3 %all-to-all-start.1 = ((bf16[16,352,128]{2,1,0:T(8,128)(2,1)}), bf16[16,352,128]{2,1,0:T(8,128)(2,1)S(1)}, u32[]{:S(2)}, u32[]{:S(2)}) async-start(bf16[16,352,128]{2,1,0:T(8,128)(2,1)} %bitcast.24), calls=%async_computation.1 | async-start | bytes 2883584 | tf_op jit(solution)/shard_map/all_to_all | solution.py:24
  127.8 173.8 %all-gather.17.cloned.1.call-start = ((), (), s32[]{:S(2)}) async-start(), calls=%async_computation.5 | async-start | bytes 2162688 | tf_op jit(solution)/shard_map/all_gather | solution.py:20
  131.1 198.3 %all-gather.19.cloned.1.call-start = ((), (), s32[]{:S(2)}) async-start(), calls=%async_computation.6 | async-start | bytes 2162688 | tf_op jit(solution)/shard_map/all_gather | solution.py:21
  131.9 328.6 %all-gather.25.cloned.1.call-start = ((), (), s32[]{:S(2)}) async-start(), calls=%async_computation.9 | async-start | bytes 17825792 | tf_op jit(solution)/shard_map/all_gather | solution.py:10
  301.5 27.9 %copy-start.7 = (bf16[352,2048]{1,0:T(8,128)(2,1)S(1)}, bf16[352,2048]{1,0:T(8,128)(2,1)}, u32[]{:S(2)}) copy-start(bf16[352,2048]{1,0:T(8,128)(2,1)} %copy_bitcast_fusion) | copy-start | bytes 4325380
  469.7 1.4 copy-start.3
  471.1 1.9 copy-start.4
  473.0 1.9 copy-start.5
  474.9 1.9 copy-start.6
Sparse Core Ops, SparseCore 0:
  10.1 28.4 all-gather.14
  40.7 25.6 all-gather.10
  68.6 25.6 all-gather.12
  96.3 25.7 all-gather.20
  124.6 151.0 all-gather.22
  277.6 23.8 all-gather.16
  303.7 25.6 all-gather.18
  334.0 126.4 all-gather.24
